TPU v7x, 256 devices: a whole 4x4x8 slice. The times are simulated.
256 devices in a mesh: kv: 16 (over y, x), tp: 16 (over z, core).
Axes of the slice: x: 4, y: 4, z: 8, core: 2. Of those that a mesh axis runs over, the one named last changes fastest.
Arguments:
- tokens: bfloat16 [1536, 4096], P('kv', 'tp'), may hold values from -20 to 20
- state: float32 [1536, 32, 4096], P('kv', 'tp'), may hold values from -4 to 4
- w_query: bfloat16 [4096, 2048], P(None, 'tp'), may hold values from -0.09375 to 0.09375
- w_key: bfloat16 [4096, 2048], P(None, 'tp'), may hold values from -0.09375 to 0.09375
- w_value: bfloat16 [4096, 2048], P(None, 'tp'), may hold values from -0.09375 to 0.09375
- w_gate: bfloat16 [4096, 2048], P(None, 'tp'), may hold values from -0.09375 to 0.09375
- w_decay: bfloat16 [4096, 32], replicated, may hold values from -0.09375 to 0.09375
- w_beta: bfloat16 [4096, 32], replicated, may hold values from -0.09375 to 0.09375
- decay_rate: float32 [32], P('tp'), may hold values from 0.03 to 3
- decay_bias: float32 [32], P('tp'), may hold values from -1 to 1
- mix_gain: float32 [4096], replicated, may hold values from 0.1 to 1.9
- out_gain: float32 [64], replicated, may hold values from 0.1 to 1.9
- w_out: bfloat16 [2048, 4096], P('tp'), may hold values from -0.125 to 0.125
- ffn_gain: float32 [4096], replicated, may hold values from 0.1 to 1.9
- w_up: bfloat16 [4096, 16384], P('tp', 'kv'), may hold values from -0.09375 to 0.09375
- w_down: bfloat16 [16384, 4096], P('kv', 'tp'), may hold values from -0.046875 to 0.046875
Outputs:
- mixed: bfloat16 [1536, 4096], P('kv', 'tp')
- new_state: float32 [1536, 32, 4096], P('kv', 'tp')
All inputs are finite; a program needn't handle non-finite values.
Results may differ from a plain program's by a relative error of at most 0.024.
Values may be sent and summed in bfloat16 or wider, within the bound.
No kernel may reach another device: no remote copies, remote signals or barrier semaphores. Data moves between devices by JAX's collectives and lax.ppermute only.
A program may use at most 64 MiB of HBM per device.

v0:
```python
import jax
import jax.numpy as jnp
from jax import lax
from jax.sharding import Mesh
from jax.sharding import PartitionSpec as P

D = 4096
HEAD_DIM = 64
TP = ("tp_0", "tp_1")
EPS = 1e-06


def sent_to_all(array, axis):
    length = lax.axis_size(axis)
    return lax.all_to_all(
        jnp.broadcast_to(array[None], (length, *array.shape)), axis, 0, 0, tiled=True
    )


def joined_along(parts, dim):
    dims = list(parts.shape[1:])
    dims[dim] *= parts.shape[0]
    return jnp.moveaxis(parts, 0, dim).reshape(dims)


def gathered_copies(array, axis, dim):
    parts = sent_to_all(array, axis)
    return joined_along(parts, dim)


def in_blocks(array, dim, length):
    before, after = (array.shape[:dim], array.shape[dim + 1 :])
    return jnp.moveaxis(array.reshape(*before, length, -1, *after), dim, 0)


def sum_at_owner(array, axis, dim):
    parts = in_blocks(array, dim, lax.axis_size(axis))
    arrived = lax.all_to_all(parts, axis, split_axis=0, concat_axis=0, tiled=True)
    return arrived.astype(jnp.float32).sum(axis=0)


def over_copies(array, axis):
    everything = sent_to_all(array, axis)
    return jnp.sum(everything, axis=0)


def scatter_pairs(array, chips, core, dim):
    sizes = (lax.axis_size(chips), lax.axis_size(core))
    parts = in_blocks(array, dim, sizes[0] * sizes[1])
    inside = parts.shape[1:]
    parts = parts.reshape(*sizes, *inside).swapaxes(0, 1).reshape(-1, *inside)
    parts = lax.psum_scatter(parts, core, scatter_dimension=0, tiled=True)
    return lax.psum_scatter(parts, chips, scatter_dimension=0, tiled=True)[0]


def unit_norm(vector):
    return vector * lax.rsqrt(jnp.sum(vector * vector, axis=-1, keepdims=True) + EPS)


def local(
    tokens,
    state,
    w_query,
    w_key,
    w_value,
    w_gate,
    w_decay,
    w_beta,
    decay_rate,
    decay_bias,
    mix_gain,
    out_gain,
    w_out,
    ffn_gain,
    w_up,
    w_down,
):
    rows = tokens.shape[0]
    width_share = tokens.shape[1]
    head_count = w_query.shape[1] // HEAD_DIM
    full_rows = gathered_copies(tokens, TP, 1)
    full_f = full_rows.astype(jnp.float32)
    normed = (
        full_f * lax.rsqrt(jnp.mean(full_f * full_f, axis=-1, keepdims=True) + EPS) * mix_gain
    ).astype(jnp.bfloat16)
    query = jnp.dot(normed, w_query, preferred_element_type=jnp.float32).reshape(
        rows, head_count, HEAD_DIM
    )
    key_proj = jnp.dot(normed, w_key, preferred_element_type=jnp.float32).reshape(
        rows, head_count, HEAD_DIM
    )
    value = jnp.dot(normed, w_value, preferred_element_type=jnp.float32).reshape(
        rows, head_count, HEAD_DIM
    )
    gate = jnp.dot(normed, w_gate, preferred_element_type=jnp.float32).reshape(
        rows, head_count, HEAD_DIM
    )
    query = unit_norm(query) * HEAD_DIM ** (-0.5)
    key_proj = unit_norm(key_proj)
    head_start = lax.axis_index(TP) * head_count
    decay_cols = lax.dynamic_slice_in_dim(w_decay, head_start, head_count, 1)
    beta_cols = lax.dynamic_slice_in_dim(w_beta, head_start, head_count, 1)
    pre_decay = jnp.dot(normed, decay_cols, preferred_element_type=jnp.float32)
    decay = jnp.exp(-decay_rate * jax.nn.softplus(pre_decay + decay_bias))
    strength = jax.nn.sigmoid(jnp.dot(normed, beta_cols, preferred_element_type=jnp.float32))
    matrix = state.reshape(rows, head_count, HEAD_DIM, HEAD_DIM) * decay[:, :, None, None]
    recalled = jnp.einsum("bhk,bhkv->bhv", key_proj, matrix, precision=lax.Precision.HIGHEST)
    delta = (value - recalled) * strength[:, :, None]
    matrix = matrix + key_proj[:, :, :, None] * delta[:, :, None, :]
    head_out = jnp.einsum("bhk,bhkv->bhv", query, matrix, precision=lax.Precision.HIGHEST)
    head_out = (
        head_out
        * lax.rsqrt(jnp.mean(head_out * head_out, axis=-1, keepdims=True) + EPS)
        * out_gain
        * jax.nn.silu(gate)
    )
    head_out = head_out.reshape(rows, head_count * HEAD_DIM).astype(jnp.bfloat16)
    partial_value = jnp.dot(head_out, w_out, preferred_element_type=jnp.float32)
    feature_start = lax.axis_index(TP) * width_share
    gain_share = lax.dynamic_slice_in_dim(ffn_gain, feature_start, width_share, 0)
    resid = tokens.astype(jnp.float32) + sum_at_owner(partial_value.astype(jnp.bfloat16), TP, 1)
    squares = over_copies(jnp.sum(resid * resid, axis=-1), TP)
    scale = lax.rsqrt(squares[:, None] / D + EPS)
    ffn_in = (resid * scale * gain_share).astype(jnp.bfloat16)
    up_part = jnp.dot(gathered_copies(ffn_in, "kv", 0), w_up, preferred_element_type=jnp.float32)
    up_share = scatter_pairs(up_part.astype(jnp.bfloat16), "tp_0", "tp_1", 0).astype(jnp.float32)
    hidden_share = jnp.square(jax.nn.relu(up_share)).astype(jnp.bfloat16)
    hidden = lax.all_gather(hidden_share, TP, axis=0, tiled=True)
    down = sum_at_owner(
        jnp.dot(hidden, w_down, preferred_element_type=jnp.float32).astype(jnp.bfloat16), "kv", 0
    )
    mixed = (resid + down).astype(jnp.bfloat16)
    return (mixed, matrix.reshape(rows, head_count, HEAD_DIM * HEAD_DIM))


def solution(mesh):
    split = Mesh(mesh.devices.reshape(mesh.shape["kv"], 8, 2), ("kv", "tp_0", "tp_1"))
    placed = (
        P("kv", TP),
        P("kv", TP, None),
        P(None, TP),
        P(None, TP),
        P(None, TP),
        P(None, TP),
        P(),
        P(),
        P(TP),
        P(TP),
        P(),
        P(),
        P(TP, None),
        P(),
        P(TP, "kv"),
        P("kv", TP),
    )
    return jax.shard_map(
        local,
        mesh=split,
        in_specs=placed,
        out_specs=(P("kv", TP), P("kv", TP, None)),
        check_vma=False,
    )
```

profile of v0, /device:TPU:1, one launch (start us, length us, event | category | flops | bytes accessed | tf_op | source)
XLA Modules:
  0.0 243.3 jit_solution(4121412433545076519)
XLA Ops:
  7.2 0.0 copy-start
  7.2 1.9 broadcast_in_dim.6
  9.1 10.0 %all-to-all-start = ((bf16[16,96,256]{2,1,0:T(8,128)(2,1)}), bf16[16,96,256]{2,1,0:T(8,128)(2,1)S(1)}, u32[]{:S(2)}, u32[]{:S(2)}) async-start(bf16[16,96,256]{2,1,0:T(8,128)(2,1)} %broadcast_in_dim.6), calls=%async_computation | async-start | bytes 1572864 | tf_op jit(solution)/shard_map/all_to_all | solution.py:15
  19.1 0.7 mul.175
  19.8 1.3 copy.69
  21.1 2.3 copy.66
  23.4 0.0 copy-done.12
  23.4 6.1 %copy.67 = f32[96,2,4096]{0,2,1:T(8,128)} copy(f32[96,2,4096]{2,1,0:T(2,128)} %param.17) | data formatting | bytes 6291456 | tf_op args[1]
  29.5 1.3 copy.70
  30.8 2.3 copy.71
  33.1 8.7 %all-to-all-done = bf16[16,96,256]{2,1,0:T(8,128)(2,1)S(1)} async-done(((bf16[16,96,256]{2,1,0:T(8,128)(2,1)}), bf16[16,96,256]{2,1,0:T(8,128)(2,1)S(1)}, u32[]{:S(2)}, u32[]{:S(2)}) %all-to-all-start) | async-done | bytes 786464 | tf_op jit(solution)/shard_map/all_to_all | solution.py:15
  41.8 0.3 fusion.5
  42.0 0.3 fusion.12
  42.3 0.4 copy.65
  42.8 0.4 reshape.142
  43.1 1.7 multiply_reduce_fusion.4
  44.8 1.7 multiply_reduce_fusion.5
  46.5 0.0 copy-start.8
  46.5 0.0 copy-start.9
  46.5 0.2 convert_bitcast_fusion
  46.7 0.2 copy.90
  46.9 0.4 copy-done.8
  47.2 1.5 fusion.11
  48.7 0.0 copy-start.2
  48.7 1.3 fusion.16
  50.1 0.6 multiply_reduce_fusion.1
  50.7 0.5 fusion.8
  51.2 0.0 copy-start.3
  51.2 0.0 copy-start.10
  51.2 3.0 %broadcast_multiply_fusion = (f32[96,2,64,64]{0,3,2,1:T(8,128)}, f32[96,2,64]{0,2,1:T(8,128)S(1)}) fusion(f32[96,2,64]{0,2,1:T(8,128)S(1)} %fusion.8, f32[96,2,64]{0,2,1:T(8,128)S(1)} %get-tuple-element.19, f32[96,2,64,64]{0,3,2,1:T(8,128)S(1)} %bitcast.55, f32[96,2]{0,1:T(2,128)S(1)} %fusion.16, f32[96,2,64]{0,2,1:T(8,128)S(1)} %get-tuple-element.18), kind=kLoop, calls=%fused_computation.11 | loop fusion | flops 3919872 | bytes 6488832 | tf_op jit(solution)/shard_map/mul | solution.py:109
  54.3 0.4 multiply_convert_fusion.3
  54.8 0.0 copy-start.6
  54.8 0.4 convolution_convert_fusion
  55.2 0.0 copy-start.7
  55.2 0.1 copy.92
  55.3 25.8 %all_to_all.26 = bf16[16,96,256]{2,1,0:T(8,128)(2,1)S(1)} all-to-all(bf16[16,96,256]{2,1,0:T(8,128)(2,1)S(1)} %bitcast.66), channel_id=1, replica_groups=mesh['kv'=16,'tp_0'=8,'tp_1'=2] {'tp_0','tp_1'}, dimensions={0} | all-to-all | bytes 1572864 | tf_op jit(solution)/shard_map/all_to_all | solution.py:38
  81.1 0.1 convert_reduce_fusion.1
  81.2 0.1 multiply_reduce_fusion.2
  81.3 0.6 broadcast_in_dim.7
  82.0 3.4 %all-to-all-start.2 = ((f32[16,1,96]{2,1,0:T(1,128)}), f32[16,1,96]{2,1,0:T(1,128)S(1)}, u32[]{:S(2)}, u32[]{:S(2)}) async-start(f32[16,1,96]{2,1,0:T(1,128)} %broadcast_in_dim.7), calls=%async_computation.2 | async-start | bytes 16384 | tf_op jit(solution)/shard_map/all_to_all | solution.py:15
  85.3 0.0 reduce-scatter.3.cloned.1.call-start
  85.4 0.8 dynamic_slice.11
  86.2 5.8 %all-to-all-done.2 = f32[16,1,96]{2,1,0:T(1,128)S(1)} async-done(((f32[16,1,96]{2,1,0:T(1,128)}), f32[16,1,96]{2,1,0:T(1,128)S(1)}, u32[]{:S(2)}, u32[]{:S(2)}) %all-to-all-start.2) | async-done | bytes 6176 | tf_op jit(solution)/shard_map/all_to_all | solution.py:15
  91.9 0.1 multiply_convert_fusion.2
  92.0 0.1 broadcast_in_dim.8
  92.1 20.1 %all_to_all.27 = bf16[16,96,256]{2,1,0:T(8,128)(2,1)S(1)} all-to-all(bf16[16,96,256]{2,1,0:T(8,128)(2,1)S(1)} %broadcast_in_dim.8), channel_id=1, replica_groups=mesh['kv'=16,'tp_0'=8,'tp_1'=2] {'kv'}, dimensions={0} | all-to-all | bytes 1572864 | tf_op jit(solution)/shard_map/all_to_all | solution.py:15
  112.2 1.0 convolution_convert_fusion.1
  113.2 2.1 copy.74
  115.3 0.0 reduce-scatter.3.cloned.1.call-update
  115.3 0.0 reduce-scatter.5.cloned.1.call-start
  115.4 10.4 %reduce-scatter.3.cloned.1.call-done = bf16[8,96,1024]{2,1,0:T(8,128)(2,1)} async-done(((bf16[16,96,1024]{2,1,0:T(8,128)(2,1)}), bf16[8,96,1024]{2,1,0:T(8,128)(2,1)}) %reduce-scatter.3.cloned.1.call-update) | async-done | bytes 1572880 | tf_op jit(solution)/shard_map/reduce_scatter | solution.py:52
  125.7 0.0 reduce-scatter.5.cloned.1.call-update
  125.8 0.0 all-gather.3.cloned.1.call-start
  125.8 40.4 %reduce-scatter.5.cloned.1.call-done = bf16[1,96,1024]{2,1,0:T(8,128)(2,1)} async-done(((bf16[8,96,1024]{2,1,0:T(8,128)(2,1)}), bf16[1,96,1024]{2,1,0:T(8,128)(2,1)}) %reduce-scatter.5.cloned.1.call-update) | async-done | bytes 196624 | tf_op jit(solution)/shard_map/reduce_scatter | solution.py:53
  166.2 1.6 multiply_convert_fusion.1
  167.9 0.0 all-gather.3.cloned.1.call-update
  167.9 44.2 %all-gather.3.cloned.1.call-done = bf16[1,1536,1024]{2,1,0:T(8,128)(2,1)} async-done(((bf16[1,96,1024]{2,1,0:T(8,128)(2,1)}), bf16[1,1536,1024]{2,1,0:T(8,128)(2,1)}) %all-gather.3.cloned.1.call-update) | async-done | bytes 3145744 | tf_op jit(solution)/shard_map/all_gather | solution.py:128
  212.1 3.8 %fusion.2 = bf16[1536,256]{1,0:T(8,128)(2,1)} fusion(bf16[1024,256]{1,0:T(8,128)(2,1)S(1)} %copy-done.11, bf16[1,1536,1024]{2,1,0:T(8,128)(2,1)} %all-gather.3.cloned.1.call-done), kind=kOutput, calls=%fused_computation.7 | convolution fusion | flops 805699584 | bytes 4456448 | tf_op jit(solution)/shard_map/dot_general | solution.py:130
  215.9 6.5 %all-to-all-start.4 = ((bf16[16,96,256]{2,1,0:T(8,128)(2,1)}), bf16[16,96,256]{2,1,0:T(8,128)(2,1)S(1)}, u32[]{:S(2)}, u32[]{:S(2)}) async-start(bf16[16,96,256]{2,1,0:T(8,128)(2,1)} %bitcast.19), calls=%async_computation.6 | async-start | bytes 1572864 | tf_op jit(solution)/shard_map/all_to_all | solution.py:38
  222.4 5.8 %bitcast_add_fusion = f32[96,2,4096]{0,2,1:T(8,128)} fusion(f32[96,2,64,64]{0,3,2,1:T(8,128)} %get-tuple-element.12, f32[96,2,4096]{0,2,1:T(8,128)} %copy.67, f32[96,2]{0,1:T(2,128)S(1)} %fusion.16), kind=kLoop, calls=%fused_computation.1 | loop fusion | flops 1572864 | bytes 9437952 | tf_op jit(solution)/shard_map/add | solution.py:109
  228.2 6.0 %copy.76 = f32[96,2,4096]{2,1,0:T(2,128)} copy(f32[96,2,4096]{0,2,1:T(8,128)} %bitcast_add_fusion) | data formatting | bytes 6291456
  234.2 1.8 all-to-all-done.4
  236.0 0.1 convert_reduce_fusion
  236.2 0.6 add_convert_fusion
  (25 shorter events, 0.1 us)
Async XLA Ops:
  7.2 47.6 %copy-start = (bf16[128,4096]{1,0:T(8,128)(2,1)S(1)}, bf16[128,4096]{1,0:T(8,128)(2,1)}, u32[]{:S(2)}) copy-start(bf16[128,4096]{1,0:T(8,128)(2,1)} %param.28) | copy-start | bytes 3145732
  7.2 12.6 %copy-start.4 = (bf16[4096,128]{1,0:T(8,128)(2,1)S(1)}, bf16[4096,128]{1,0:T(8,128)(2,1)}, u32[]{:S(2)}) copy-start(bf16[4096,128]{1,0:T(8,128)(2,1)} %param.19) | copy-start | bytes 3145732
  7.2 16.2 %copy-start.12 = (f32[2]{0:T(128)S(1)}, f32[2]{0:T(128)}, u32[]{:S(2)}) copy-start(f32[2]{0:T(128)} %param.24) | copy-start | bytes 28
  9.1 32.7 %all-to-all-start = ((bf16[16,96,256]{2,1,0:T(8,128)(2,1)}), bf16[16,96,256]{2,1,0:T(8,128)(2,1)S(1)}, u32[]{:S(2)}, u32[]{:S(2)}) async-start(bf16[16,96,256]{2,1,0:T(8,128)(2,1)} %broadcast_in_dim.6), calls=%async_computation | async-start | bytes 1572864 | tf_op jit(solution)/shard_map/all_to_all | solution.py:15
  23.4 6.1 %copy-start.5 = (bf16[4096,128]{1,0:T(8,128)(2,1)S(1)}, bf16[4096,128]{1,0:T(8,128)(2,1)}, u32[]{:S(2)}) copy-start(bf16[4096,128]{1,0:T(8,128)(2,1)} %param.20) | copy-start | bytes 3145732
  46.5 0.7 copy-start.8
  46.5 2.2 copy-start.9
  46.7 3.4 %copy-start.1 = (f32[96,2,4096]{0,2,1:T(8,128)S(1)}, f32[96,2,4096]{0,2,1:T(8,128)}, u32[]{:S(2)}) copy-start(f32[96,2,4096]{0,2,1:T(8,128)} %copy.67) | copy-start | bytes 9437188
  48.7 2.0 copy-start.2
  51.2 3.1 %copy-start.3 = (bf16[4096,128]{0,1:T(8,128)(2,1)S(1)}, bf16[4096,128]{0,1:T(8,128)(2,1)}, u32[]{:S(2)}) copy-start(bf16[4096,128]{0,1:T(8,128)(2,1)} %copy.71) | copy-start | bytes 3145732
  51.2 3.1 %copy-start.10 = (f32[64]{0:T(128)S(1)}, f32[64]{0:T(128)}, u32[]{:S(2)}) copy-start(f32[64]{0:T(128)} %param.27) | copy-start | bytes 772
  54.8 26.5 %copy-start.6 = (bf16[96,256]{1,0:T(8,128)(2,1)S(1)}, bf16[96,256]{1,0:T(8,128)(2,1)}, u32[]{:S(2)}) copy-start(bf16[96,256]{1,0:T(8,128)(2,1)} %param.16) | copy-start | bytes 147460
  55.2 57.0 %copy-start.7 = (bf16[256,1024]{1,0:T(8,128)(2,1)S(1)}, bf16[256,1024]{1,0:T(8,128)(2,1)}, u32[]{:S(2)}) copy-start(bf16[256,1024]{1,0:T(8,128)(2,1)} %param.30) | copy-start | bytes 1572868
  82.0 10.0 %all-to-all-start.2 = ((f32[16,1,96]{2,1,0:T(1,128)}), f32[16,1,96]{2,1,0:T(1,128)S(1)}, u32[]{:S(2)}, u32[]{:S(2)}) async-start(f32[16,1,96]{2,1,0:T(1,128)} %broadcast_in_dim.7), calls=%async_computation.2 | async-start | bytes 16384 | tf_op jit(solution)/shard_map/all_to_all | solution.py:15
  85.3 40.4 %reduce-scatter.3.cloned.1.call-start = ((), (), s32[]{:S(2)}) async-start(), calls=%async_computation.7 | async-start | bytes 4718592 | tf_op jit(solution)/shard_map/reduce_scatter | solution.py:52
  115.3 96.8 %copy-start.11 = (bf16[1024,256]{1,0:T(8,128)(2,1)S(1)}, bf16[1024,256]{1,0:T(8,128)(2,1)}, u32[]{:S(2)}) copy-start(bf16[1024,256]{1,0:T(8,128)(2,1)} %param.31) | copy-start | bytes 1572868
  115.3 50.9 %reduce-scatter.5.cloned.1.call-start = ((), (), s32[]{:S(2)}) async-start(), calls=%async_computation.8 | async-start | bytes 1769472 | tf_op jit(solution)/shard_map/reduce_scatter | solution.py:53
  125.8 86.4 %all-gather.3.cloned.1.call-start = ((), (), s32[]{:S(2)}) async-start(), calls=%async_computation.9 | async-start | bytes 3342336 | tf_op jit(solution)/shard_map/all_gather | solution.py:128
  215.9 20.2 %all-to-all-start.4 = ((bf16[16,96,256]{2,1,0:T(8,128)(2,1)}), bf16[16,96,256]{2,1,0:T(8,128)(2,1)S(1)}, u32[]{:S(2)}, u32[]{:S(2)}) async-start(bf16[16,96,256]{2,1,0:T(8,128)(2,1)} %bitcast.19), calls=%async_computation.6 | async-start | bytes 1572864 | tf_op jit(solution)/shard_map/all_to_all | solution.py:38
Sparse Core Ops, SparseCore 0:
  115.5 10.2 reduce-scatter.2
  128.3 37.8 reduce-scatter.4
  168.6 43.4 all-gather.2
where the time goes:
time: 244 us; the launch traced here: 243 us
  waiting for transfers between devices  111 us (45%)
  blocking collectives  45.9 us (19%)
  local copies, waits for them, and re-layouts  26.8 us (11%)
  starting transfers between devices  20 us (8%)
  between operations  14 us (6%)
  other arithmetic  12.9 us (5%)
  matrix products  12.2 us (5%)
    all_gather x1, waiting for transfers between devices, local(): hidden = lax.all_gather(hidden_share, TP, axis=0, tiled=True)  44.2 us
    reduce_scatter x1, waiting for transfers between devices, scatter_pairs(): return lax.psum_scatter(parts, chips, scatter_dimension=0, tiled=True)[0]  40.4 us
    all_to_all x1, blocking collectives, sum_at_owner(): lax.all_to_all(parts, axis, split_axis=0, concat_axis=0, tiled=True)  25.8 us
    all_to_all x1, blocking collectives, sent_to_all(): lax.all_to_all(jnp.broadcast_to(array[None], (length, *array.shape)), axi...  20.1 us
    unnamed x32, local copies, waits for them, and re-layouts  19.7 us
    all_to_all x2, waiting for transfers between devices, sent_to_all(): lax.all_to_all(jnp.broadcast_to(array[None], (length, *array.shape)), axi...  14.5 us
    all_to_all x2, starting transfers between devices, sent_to_all(): lax.all_to_all(jnp.broadcast_to(array[None], (length, *array.shape)), axi...  13.3 us
    reduce_scatter x1, waiting for transfers between devices, scatter_pairs(): parts = lax.psum_scatter(parts, core, scatter_dimension=0, tiled=True)  10.4 us
  transfers between devices with their start and end apart: 6, of which 6 were waited for; matrix products, arithmetic and copies ran while one was open for 11% of the time, Pallas kernels for 0%

commit v1 on v0

--- a/solution.py
+++ b/solution.py
@@ -125,7 +125,9 @@
     up_part = jnp.dot(gathered_copies(ffn_in, "kv", 0), w_up, preferred_element_type=jnp.float32)
     up_share = scatter_pairs(up_part.astype(jnp.bfloat16), "tp_0", "tp_1", 0).astype(jnp.float32)
     hidden_share = jnp.square(jax.nn.relu(up_share)).astype(jnp.bfloat16)
-    hidden = lax.all_gather(hidden_share, TP, axis=0, tiled=True)
+    hidden = jnp.concatenate(
+        lax.all_to_all(jnp.stack([hidden_share] * lax.axis_size(TP)), TP, 0, 0), axis=0
+    )
     down = sum_at_owner(
         jnp.dot(hidden, w_down, preferred_element_type=jnp.float32).astype(jnp.bfloat16), "kv", 0
     )

time: 244 us -> 281 us (1.15)
  blocking collectives: 45.9 us -> 128 us
  waiting for transfers between devices: 111 us -> 68.1 us
    all_to_all x0 -> x1, blocking collectives: none -> 82.3 us  [local(): lax.all_to_all(jnp.stack([hidden_share] * lax.axis_size(TP)), TP, 0, 0)]
    all_gather x1 -> x0, waiting for transfers between devices: 44.2 us -> none  [local(): hidden = lax.all_gather(hidden_share, TP, axis=0, tiled=True)]
  transfers between devices with their start and end apart: 6 -> 5, of which waited for: 6 -> 5; matrix products, arithmetic and copies ran while one was open for 11% -> 9% of each run, Pallas kernels for 0% -> 0%
where the time goes in v1:
time: 281 us
  blocking collectives  128 us (46%)
  waiting for transfers between devices  68.1 us (24%)
  local copies, waits for them, and re-layouts  27.2 us (10%)
  starting transfers between devices  19.9 us (7%)
  between operations  14.4 us (5%)
  other arithmetic  12.2 us (4%)
  matrix products  10.4 us (4%)
    all_to_all x1, blocking collectives, local(): lax.all_to_all(jnp.stack([hidden_share] * lax.axis_size(TP)), TP, 0, 0)  82.3 us
    reduce_scatter x1, waiting for transfers between devices, scatter_pairs(): return lax.psum_scatter(parts, chips, scatter_dimension=0, tiled=True)[0]  40.5 us
    all_to_all x1, blocking collectives, sum_at_owner(): lax.all_to_all(parts, axis, split_axis=0, concat_axis=0, tiled=True)  25.8 us
    all_to_all x1, blocking collectives, sent_to_all(): lax.all_to_all(jnp.broadcast_to(array[None], (length, *array.shape)), axi...  20.1 us
    unnamed x32, local copies, waits for them, and re-layouts  19.7 us
    all_to_all x2, waiting for transfers between devices, sent_to_all(): lax.all_to_all(jnp.broadcast_to(array[None], (length, *array.shape)), axi...  14.5 us
    all_to_all x2, starting transfers between devices, sent_to_all(): lax.all_to_all(jnp.broadcast_to(array[None], (length, *array.shape)), axi...  13.3 us
    reduce_scatter x1, waiting for transfers between devices, scatter_pairs(): parts = lax.psum_scatter(parts, core, scatter_dimension=0, tiled=True)  10.4 us
  transfers between devices with their start and end apart: 5, of which 5 were waited for; matrix products, arithmetic and copies ran while one was open for 9% of the time, Pallas kernels for 0%

profile of v1, /device:TPU:1, one launch (start us, length us, event | category | flops | bytes accessed | tf_op | source)
XLA Modules:
  0.0 280.5 jit_solution(12561283472467367502)
XLA Ops:
  7.2 0.0 copy-start
  7.2 1.9 broadcast_in_dim.6
  9.1 10.0 %all-to-all-start = ((bf16[16,96,256]{2,1,0:T(8,128)(2,1)}), bf16[16,96,256]{2,1,0:T(8,128)(2,1)S(1)}, u32[]{:S(2)}, u32[]{:S(2)}) async-start(bf16[16,96,256]{2,1,0:T(8,128)(2,1)} %broadcast_in_dim.6), calls=%async_computation | async-start | bytes 1572864 | tf_op jit(solution)/shard_map/all_to_all | solution.py:15
  19.1 0.7 mul.175
  19.8 1.3 copy.69
  21.1 2.3 copy.66
  23.4 0.0 copy-done.12
  23.4 6.1 %copy.67 = f32[96,2,4096]{0,2,1:T(8,128)} copy(f32[96,2,4096]{2,1,0:T(2,128)} %param.17) | data formatting | bytes 6291456 | tf_op args[1]
  29.5 1.3 copy.70
  30.8 2.3 copy.71
  33.1 8.7 %all-to-all-done = bf16[16,96,256]{2,1,0:T(8,128)(2,1)S(1)} async-done(((bf16[16,96,256]{2,1,0:T(8,128)(2,1)}), bf16[16,96,256]{2,1,0:T(8,128)(2,1)S(1)}, u32[]{:S(2)}, u32[]{:S(2)}) %all-to-all-start) | async-done | bytes 786464 | tf_op jit(solution)/shard_map/all_to_all | solution.py:15
  41.8 0.3 fusion
  42.0 0.3 fusion.7
  42.3 0.4 copy.65
  42.8 0.4 reshape.141
  43.1 1.7 multiply_reduce_fusion.4
  44.8 1.7 multiply_reduce_fusion.5
  46.5 0.0 copy-start.8
  46.5 0.0 copy-start.9
  46.5 0.2 convert_bitcast_fusion
  46.7 0.2 copy.90
  46.9 0.4 copy-done.8
  47.2 1.5 fusion.6
  48.7 0.0 copy-start.2
  48.7 1.3 fusion.12
  50.1 0.6 multiply_reduce_fusion.1
  50.7 0.5 fusion.3
  51.2 0.0 copy-start.3
  51.2 0.0 copy-start.10
  51.2 3.0 %broadcast_multiply_fusion = (f32[96,2,64,64]{0,3,2,1:T(8,128)}, f32[96,2,64]{0,2,1:T(8,128)S(1)}) fusion(f32[96,2,64]{0,2,1:T(8,128)S(1)} %fusion.3, f32[96,2,64]{0,2,1:T(8,128)S(1)} %get-tuple-element.19, f32[96,2,64,64]{0,3,2,1:T(8,128)S(1)} %bitcast.54, f32[96,2]{0,1:T(2,128)S(1)} %fusion.12, f32[96,2,64]{0,2,1:T(8,128)S(1)} %get-tuple-element.18), kind=kLoop, calls=%fused_computation.9 | loop fusion | flops 3919872 | bytes 6488832 | tf_op jit(solution)/shard_map/mul | solution.py:109
  54.3 0.4 multiply_convert_fusion.3
  54.8 0.0 copy-start.6
  54.8 0.4 convolution_convert_fusion
  55.2 0.0 copy-start.7
  55.2 0.1 copy.92
  55.3 25.8 %all_to_all.31 = bf16[16,96,256]{2,1,0:T(8,128)(2,1)S(1)} all-to-all(bf16[16,96,256]{2,1,0:T(8,128)(2,1)S(1)} %bitcast.66), channel_id=1, replica_groups=mesh['kv'=16,'tp_0'=8,'tp_1'=2] {'tp_0','tp_1'}, dimensions={0} | all-to-all | bytes 1572864 | tf_op jit(solution)/shard_map/all_to_all | solution.py:38
  81.1 0.1 convert_reduce_fusion.1
  81.2 0.1 multiply_reduce_fusion.2
  81.3 0.6 broadcast_in_dim.7
  82.0 3.4 %all-to-all-start.2 = ((f32[16,1,96]{2,1,0:T(1,128)}), f32[16,1,96]{2,1,0:T(1,128)S(1)}, u32[]{:S(2)}, u32[]{:S(2)}) async-start(f32[16,1,96]{2,1,0:T(1,128)} %broadcast_in_dim.7), calls=%async_computation.2 | async-start | bytes 16384 | tf_op jit(solution)/shard_map/all_to_all | solution.py:15
  85.3 0.0 reduce-scatter.3.cloned.1.call-start
  85.4 0.8 dynamic_slice.11
  86.2 5.8 %all-to-all-done.2 = f32[16,1,96]{2,1,0:T(1,128)S(1)} async-done(((f32[16,1,96]{2,1,0:T(1,128)}), f32[16,1,96]{2,1,0:T(1,128)S(1)}, u32[]{:S(2)}, u32[]{:S(2)}) %all-to-all-start.2) | async-done | bytes 6176 | tf_op jit(solution)/shard_map/all_to_all | solution.py:15
  91.9 0.1 multiply_convert_fusion.2
  92.0 0.1 broadcast_in_dim.8
  92.1 20.1 %all_to_all.32 = bf16[16,96,256]{2,1,0:T(8,128)(2,1)S(1)} all-to-all(bf16[16,96,256]{2,1,0:T(8,128)(2,1)S(1)} %broadcast_in_dim.8), channel_id=1, replica_groups=mesh['kv'=16,'tp_0'=8,'tp_1'=2] {'kv'}, dimensions={0} | all-to-all | bytes 1572864 | tf_op jit(solution)/shard_map/all_to_all | solution.py:15
  112.2 1.0 convolution_convert_fusion.1
  113.2 2.1 copy.74
  115.3 0.0 reduce-scatter.3.cloned.1.call-update
  115.3 0.0 reduce-scatter.5.cloned.1.call-start
  115.4 10.4 %reduce-scatter.3.cloned.1.call-done = bf16[8,96,1024]{2,1,0:T(8,128)(2,1)} async-done(((bf16[16,96,1024]{2,1,0:T(8,128)(2,1)}), bf16[8,96,1024]{2,1,0:T(8,128)(2,1)}) %reduce-scatter.3.cloned.1.call-update) | async-done | bytes 1572880 | tf_op jit(solution)/shard_map/reduce_scatter | solution.py:52
  125.7 0.0 reduce-scatter.5.cloned.1.call-update
  125.8 40.5 %reduce-scatter.5.cloned.1.call-done = bf16[1,96,1024]{2,1,0:T(8,128)(2,1)} async-done(((bf16[8,96,1024]{2,1,0:T(8,128)(2,1)}), bf16[1,96,1024]{2,1,0:T(8,128)(2,1)}) %reduce-scatter.5.cloned.1.call-update) | async-done | bytes 196624 | tf_op jit(solution)/shard_map/reduce_scatter | solution.py:53
  166.2 1.0 fusion.8
  167.2 0.4 stack.5
  167.6 0.0 copy-start.11
  167.6 82.3 %all_to_all.33 = bf16[16,96,1024]{2,1,0:T(8,128)(2,1)S(1)} all-to-all(bf16[16,96,1024]{2,1,0:T(8,128)(2,1)S(1)} %stack.5), channel_id=1, replica_groups=mesh['kv'=16,'tp_0'=8,'tp_1'=2] {'tp_0','tp_1'}, dimensions={0} | all-to-all | bytes 6291456 | tf_op jit(solution)/shard_map/all_to_all | solution.py:129
  249.9 2.0 convolution_convert_fusion.2
  251.8 6.5 %all-to-all-start.5 = ((bf16[16,96,256]{2,1,0:T(8,128)(2,1)}), bf16[16,96,256]{2,1,0:T(8,128)(2,1)S(1)}, u32[]{:S(2)}, u32[]{:S(2)}) async-start(bf16[16,96,256]{2,1,0:T(8,128)(2,1)} %bitcast.20), calls=%async_computation.7 | async-start | bytes 1572864 | tf_op jit(solution)/shard_map/all_to_all | solution.py:38
  258.3 5.8 %bitcast_add_fusion = f32[96,2,4096]{0,2,1:T(8,128)} fusion(f32[96,2,64,64]{0,3,2,1:T(8,128)} %get-tuple-element.12, f32[96,2,4096]{0,2,1:T(8,128)} %copy.67, f32[96,2]{0,1:T(2,128)S(1)} %fusion.12), kind=kLoop, calls=%fused_computation.1 | loop fusion | flops 1572864 | bytes 9437952 | tf_op jit(solution)/shard_map/add | solution.py:109
  264.1 6.0 %copy.76 = f32[96,2,4096]{2,1,0:T(2,128)} copy(f32[96,2,4096]{0,2,1:T(8,128)} %bitcast_add_fusion) | data formatting | bytes 6291456
  270.1 2.8 %all-to-all-done.5 = bf16[16,96,256]{2,1,0:T(8,128)(2,1)S(1)} async-done(((bf16[16,96,256]{2,1,0:T(8,128)(2,1)}), bf16[16,96,256]{2,1,0:T(8,128)(2,1)S(1)}, u32[]{:S(2)}, u32[]{:S(2)}) %all-to-all-start.5) | async-done | bytes 786464 | tf_op jit(solution)/shard_map/all_to_all | solution.py:38
  272.9 0.1 convert_reduce_fusion
  273.0 0.6 add_convert_fusion
  (24 shorter events, 0.1 us)
Async XLA Ops:
  7.2 47.6 %copy-start = (bf16[128,4096]{1,0:T(8,128)(2,1)S(1)}, bf16[128,4096]{1,0:T(8,128)(2,1)}, u32[]{:S(2)}) copy-start(bf16[128,4096]{1,0:T(8,128)(2,1)} %param.28) | copy-start | bytes 3145732
  7.2 12.6 %copy-start.4 = (bf16[4096,128]{1,0:T(8,128)(2,1)S(1)}, bf16[4096,128]{1,0:T(8,128)(2,1)}, u32[]{:S(2)}) copy-start(bf16[4096,128]{1,0:T(8,128)(2,1)} %param.19) | copy-start | bytes 3145732
  7.2 16.2 %copy-start.12 = (f32[2]{0:T(128)S(1)}, f32[2]{0:T(128)}, u32[]{:S(2)}) copy-start(f32[2]{0:T(128)} %param.24) | copy-start | bytes 28
  9.1 32.7 %all-to-all-start = ((bf16[16,96,256]{2,1,0:T(8,128)(2,1)}), bf16[16,96,256]{2,1,0:T(8,128)(2,1)S(1)}, u32[]{:S(2)}, u32[]{:S(2)}) async-start(bf16[16,96,256]{2,1,0:T(8,128)(2,1)} %broadcast_in_dim.6), calls=%async_computation | async-start | bytes 1572864 | tf_op jit(solution)/shard_map/all_to_all | solution.py:15
  23.4 6.1 %copy-start.5 = (bf16[4096,128]{1,0:T(8,128)(2,1)S(1)}, bf16[4096,128]{1,0:T(8,128)(2,1)}, u32[]{:S(2)}) copy-start(bf16[4096,128]{1,0:T(8,128)(2,1)} %param.20) | copy-start | bytes 3145732
  46.5 0.7 copy-start.8
  46.5 2.2 copy-start.9
  46.7 3.4 %copy-start.1 = (f32[96,2,4096]{0,2,1:T(8,128)S(1)}, f32[96,2,4096]{0,2,1:T(8,128)}, u32[]{:S(2)}) copy-start(f32[96,2,4096]{0,2,1:T(8,128)} %copy.67) | copy-start | bytes 9437188
  48.7 2.0 copy-start.2
  51.2 3.1 %copy-start.3 = (bf16[4096,128]{0,1:T(8,128)(2,1)S(1)}, bf16[4096,128]{0,1:T(8,128)(2,1)}, u32[]{:S(2)}) copy-start(bf16[4096,128]{0,1:T(8,128)(2,1)} %copy.71) | copy-start | bytes 3145732
  51.2 3.1 %copy-start.10 = (f32[64]{0:T(128)S(1)}, f32[64]{0:T(128)}, u32[]{:S(2)}) copy-start(f32[64]{0:T(128)} %param.27) | copy-start | bytes 772
  54.8 26.5 %copy-start.6 = (bf16[96,256]{1,0:T(8,128)(2,1)S(1)}, bf16[96,256]{1,0:T(8,128)(2,1)}, u32[]{:S(2)}) copy-start(bf16[96,256]{1,0:T(8,128)(2,1)} %param.16) | copy-start | bytes 147460
  55.2 57.0 %copy-start.7 = (bf16[256,1024]{1,0:T(8,128)(2,1)S(1)}, bf16[256,1024]{1,0:T(8,128)(2,1)}, u32[]{:S(2)}) copy-start(bf16[256,1024]{1,0:T(8,128)(2,1)} %param.30) | copy-start | bytes 1572868
  82.0 10.0 %all-to-all-start.2 = ((f32[16,1,96]{2,1,0:T(1,128)}), f32[16,1,96]{2,1,0:T(1,128)S(1)}, u32[]{:S(2)}, u32[]{:S(2)}) async-start(f32[16,1,96]{2,1,0:T(1,128)} %broadcast_in_dim.7), calls=%async_computation.2 | async-start | bytes 16384 | tf_op jit(solution)/shard_map/all_to_all | solution.py:15
  85.3 40.4 %reduce-scatter.3.cloned.1.call-start = ((), (), s32[]{:S(2)}) async-start(), calls=%async_computation.8 | async-start | bytes 4718592 | tf_op jit(solution)/shard_map/reduce_scatter | solution.py:52
  115.3 50.9 %reduce-scatter.5.cloned.1.call-start = ((), (), s32[]{:S(2)}) async-start(), calls=%async_computation.9 | async-start | bytes 1769472 | tf_op jit(solution)/shard_map/reduce_scatter | solution.py:53
  167.6 82.3 %copy-start.11 = (bf16[1024,256]{1,0:T(8,128)(2,1)S(1)}, bf16[1024,256]{1,0:T(8,128)(2,1)}, u32[]{:S(2)}) copy-start(bf16[1024,256]{1,0:T(8,128)(2,1)} %param.31) | copy-start | bytes 1572868
  251.8 21.1 %all-to-all-start.5 = ((bf16[16,96,256]{2,1,0:T(8,128)(2,1)}), bf16[16,96,256]{2,1,0:T(8,128)(2,1)S(1)}, u32[]{:S(2)}, u32[]{:S(2)}) async-start(bf16[16,96,256]{2,1,0:T(8,128)(2,1)} %bitcast.20), calls=%async_computation.7 | async-start | bytes 1572864 | tf_op jit(solution)/shard_map/all_to_all | solution.py:38
Sparse Core Ops, SparseCore 0:
  115.5 10.2 reduce-scatter.2
  128.3 37.8 reduce-scatter.4
